TPU v7x, 32 devices: a whole 2x2x4 slice. The times are simulated.
32 devices in a mesh: sp: 8 (over z, x), tp: 4 (over y, core).
Axes of the slice: x: 2, y: 2, z: 4, core: 2. Of those that a mesh axis runs over, the one named last changes fastest.
Arguments:
- tokens: bfloat16 [3072, 2048], P(('sp', 'tp')), may hold values from -6 to 6
- norm_gain: float32 [2048], replicated, may hold values from 0.1 to 1.9
- w_recept: bfloat16 [2048, 1024], P(None, 'tp'), may hold values from -0.125 to 0.125
- w_key: bfloat16 [2048, 1024], P(None, 'tp'), may hold values from -0.125 to 0.125
- w_value: bfloat16 [2048, 1024], P(None, 'tp'), may hold values from -0.125 to 0.125
- w_decay: bfloat16 [2048, 1024], P(None, 'tp'), may hold values from -0.125 to 0.125
- w_rate: bfloat16 [2048, 1024], P(None, 'tp'), may hold values from -0.125 to 0.125
- w_gate: bfloat16 [2048, 1024], P(None, 'tp'), may hold values from -0.125 to 0.125
- shift_mix: float32 [3, 1024], P(None, 'tp'), may hold values from 0 to 1
- decay_base: float32 [1024], P('tp'), may hold values from -16 to -2
- rate_base: float32 [1024], P('tp'), may hold values from -10 to 1
- decay_drift: float32 [3072], P('sp'), may hold values from -2 to 2, as said below
- group_gain: float32 [1024], P('tp'), may hold values from 0.1 to 1.9
- initial_state: float32 [16, 64, 64], P('tp'), may hold values from -240 to 240
- w_out: bfloat16 [1024, 2048], replicated, may hold values from -0.1875 to 0.1875
Outputs:
- out: bfloat16 [3072, 2048], P(('sp', 'tp'))
Inputs may be any that keep to these rules, and one draw needn't show every extreme that they name: `decay_drift`: constant over aligned runs of 64 positions.
All inputs are finite; a program needn't handle non-finite values.
Results may differ from a plain program's by a relative error of at most 0.0083.
Values may be sent and summed in bfloat16 or wider, within the bound.
A program may use at most 128 MiB of HBM per device.

v0:
```python
import jax
import jax.numpy as jnp
from jax import lax
from jax.sharding import PartitionSpec as P

HEAD = 64
BLOCK = 64
norm_floor = 0.5
group_floor = 1.0
highest = lax.Precision.HIGHEST


def shifted_2(block, axis, distance):
    devices = range(lax.axis_size(axis))
    route = [(i - distance, i) for i in devices if i - distance in devices]
    return lax.ppermute(block, axis, route)


def carried_in(value, axis, join, neutral):
    count, mine = (lax.axis_size(axis), lax.axis_index(axis))
    pieces = jax.tree.map(lambda part: lax.all_gather(part, axis), value)
    running = jax.tree.map(
        lambda part, zero: jnp.full_like(part, 0) + jnp.asarray(zero, part.dtype), value, neutral
    )

    def turn(position, running):
        longer = join(running, jax.tree.map(lambda part: part[position], pieces))
        return jax.tree.map(lambda new, old: jnp.where(position < mine, new, old), longer, running)

    return lax.fori_loop(0, count - 1, turn, running)


def block_masks(width):
    places = lax.broadcasted_iota(jnp.int32, (width, width), 0)
    others = lax.broadcasted_iota(jnp.int32, (width, width), 1)
    return (others < places, others <= places)


def pair_dots(left, right):
    return jnp.einsum("bhtn,bhsn->bhts", left, right, precision=highest)


def chain_product(first, second):
    return jnp.einsum("hij,hjk->hik", first, second, precision=highest)


def prepare_blocks(streams):
    recept, decay, key, value, unit, rate = streams
    width = recept.shape[2]
    size = recept.shape[3]
    strict, inclusive = block_masks(width)
    logs = jnp.log(decay)
    running = jnp.cumsum(logs, axis=2)
    through = jnp.exp(running)
    until = jnp.exp(running - logs)
    alpha = -unit * until
    beta = unit * rate / through
    key_scaled = key / through
    recept_scaled = recept * through
    lower_ab = jnp.where(strict, pair_dots(alpha, beta), 0.0)
    lower_ak = jnp.where(strict, pair_dots(alpha, key_scaled), 0.0)
    system = jnp.eye(width, dtype=jnp.float32) - lower_ab
    targets = jnp.concatenate(
        [alpha, jnp.einsum("bhts,bhsr->bhtr", lower_ak, value, precision=highest)], axis=3
    )
    solved = jax.scipy.linalg.solve_triangular(system, targets, lower=True, unit_diagonal=True)
    solved_alpha = solved[..., :size]
    solved_value = solved[..., size:]
    final = through[:, :, -1:, :]
    beta_final = beta * final
    key_final = key_scaled * final
    transition = jnp.eye(size, dtype=jnp.float32) * final + jnp.einsum(
        "bhtm,bhtn->bhmn", solved_alpha, beta_final, precision=highest
    )
    added = jnp.einsum("bhtr,bhtn->bhrn", solved_value, beta_final, precision=highest) + jnp.einsum(
        "bhtr,bhtn->bhrn", value, key_final, precision=highest
    )
    upper_b = jnp.where(inclusive, pair_dots(recept_scaled, beta), 0.0)
    upper_k = jnp.where(inclusive, pair_dots(recept_scaled, key_scaled), 0.0)
    reads = recept_scaled + jnp.einsum("bhts,bhsn->bhtn", upper_b, solved_alpha, precision=highest)
    fixed_out = jnp.einsum(
        "bhts,bhsr->bhtr", upper_b, solved_value, precision=highest
    ) + jnp.einsum("bhts,bhsr->bhtr", upper_k, value, precision=highest)
    return (transition, added, reads, fixed_out)


def run_blocks(start, prepared, extra_rows):
    transition, added, reads, fixed_out = prepared
    added = jnp.concatenate(
        [added, jnp.zeros(added.shape[:2] + (extra_rows, added.shape[3]), jnp.float32)], axis=2
    )
    fixed_out = jnp.concatenate(
        [fixed_out, jnp.zeros(fixed_out.shape[:3] + (extra_rows,), jnp.float32)], axis=3
    )

    def block_step(state, inputs):
        trans_now, added_now, reads_now, fixed_now = inputs
        new_state = jnp.einsum("hrm,hmn->hrn", state, trans_now, precision=highest) + added_now
        readout = jnp.einsum("htn,hrn->htr", reads_now, state, precision=highest) + fixed_now
        return (new_state, readout)

    return lax.scan(block_step, start, (transition, added, reads, fixed_out))


def per_device(
    tokens,
    norm_gain,
    w_recept,
    w_key,
    w_value,
    w_decay,
    w_rate,
    w_gate,
    shift_mix,
    decay_base,
    rate_base,
    decay_drift,
    group_gain,
    initial_state,
    w_out,
):
    tok_float = tokens.astype(jnp.float32)
    normed = (
        tok_float
        * lax.rsqrt(jnp.mean(tok_float * tok_float, axis=-1, keepdims=True) + norm_floor)
        * norm_gain
    ).astype(jnp.bfloat16)
    weights = (w_recept, w_key, w_value, w_decay, w_rate, w_gate)
    piece = lax.all_gather(normed, "tp", axis=0, tiled=True)
    projected = jnp.stack(
        [
            jnp.dot(piece, weight, preferred_element_type=jnp.float32).astype(jnp.bfloat16)
            for weight in weights
        ],
        axis=0,
    )
    edge_rows = projected[0:3, -1:, :]
    earlier_rows = shifted_2(edge_rows, "sp", 1)
    current = projected[0:3].astype(jnp.float32)
    earlier = jnp.concatenate([earlier_rows.astype(jnp.float32), current[:, :-1]], axis=1)
    shifted = current + (earlier - current) * shift_mix[:, None, :]
    recept, key, value = (shifted[0], shifted[1], shifted[2])
    level = decay_base + projected[3].astype(jnp.float32) + decay_drift[:, None]
    decay = jnp.exp(-jnp.exp(-jax.nn.softplus(-level) - 0.5))
    rate = jax.nn.sigmoid(rate_base + projected[4].astype(jnp.float32))
    gate = jax.nn.sigmoid(projected[5].astype(jnp.float32))
    seq_rows, local_width = recept.shape
    local_heads = local_width // HEAD
    block_count = seq_rows // BLOCK

    def blocked(array):
        return array.reshape(block_count, BLOCK, local_heads, HEAD).transpose(0, 2, 1, 3)

    key_heads = key.reshape(seq_rows, local_heads, HEAD)
    unit = key_heads * lax.rsqrt(jnp.sum(key_heads * key_heads, axis=-1, keepdims=True) + 1.0)
    streams = (
        blocked(recept),
        blocked(decay),
        blocked(key),
        blocked(value),
        blocked(unit.reshape(seq_rows, local_width)),
        blocked(rate),
    )
    prepared = prepare_blocks(streams)
    identity = jnp.broadcast_to(jnp.eye(HEAD, dtype=jnp.float32), (local_heads, HEAD, HEAD))
    empty = jnp.zeros((local_heads, HEAD, HEAD), jnp.float32)
    start_state = jnp.concatenate([empty, identity], axis=1)

    def combine(earlier_pair, later_pair):
        first_map, first_add = earlier_pair
        second_map, second_add = later_pair
        return (
            chain_product(first_map, second_map),
            chain_product(first_add, second_map) + second_add,
        )

    stretch, readout = run_blocks(start_state, prepared, HEAD)
    prefix_map, prefix_add = carried_in(
        (stretch[:, HEAD:], stretch[:, :HEAD]), "sp", combine, (identity, empty)
    )
    carried = chain_product(initial_state, prefix_map) + prefix_add
    mixed = readout[..., :HEAD] + jnp.einsum(
        "bhtj,hvj->bhtv", readout[..., HEAD:], carried, precision=highest
    )
    center = mixed - jnp.mean(mixed, axis=-1, keepdims=True)
    spread = jnp.mean(center * center, axis=-1, keepdims=True)
    gains = group_gain.reshape(local_heads, HEAD)[None, :, None, :]
    scaled = center * lax.rsqrt(spread + group_floor) * gains
    flat = scaled.transpose(0, 2, 1, 3).reshape(seq_rows, local_width)
    gated = (flat * gate).astype(jnp.bfloat16)
    token_rows = lax.all_to_all(gated, "tp", split_axis=0, concat_axis=1, tiled=True)
    result = jnp.dot(token_rows, w_out, preferred_element_type=jnp.float32).astype(jnp.bfloat16)
    return result


def solution(mesh):
    return jax.shard_map(
        per_device,
        mesh=mesh,
        in_specs=(
            P(("sp", "tp"), None),
            P(),
            P(None, "tp"),
            P(None, "tp"),
            P(None, "tp"),
            P(None, "tp"),
            P(None, "tp"),
            P(None, "tp"),
            P(None, "tp"),
            P("tp"),
            P("tp"),
            P("sp"),
            P("tp"),
            P("tp", None, None),
            P(),
        ),
        out_specs=P(("sp", "tp"), None),
        check_vma=False,
    )
```

profile of v0, /device:TPU:0, one launch (start us, length us, event | category | flops | bytes accessed | tf_op | source)
XLA Modules:
  0.0 325.6 jit_solution(3846499401676920296)
XLA Ops:
  6.5 1.3 fusion.51
  7.8 1.9 fusion.53
  13.2 19.1 %all-gather.4.cloned.1.call-done = bf16[384,2048]{1,0:T(8,128)(2,1)} async-done(((bf16[96,2048]{1,0:T(8,128)(2,1)}), bf16[384,2048]{1,0:T(8,128)(2,1)}) %all-gather.4.cloned.1.call-update) | async-done | bytes 1572880 | tf_op jit(solution)/shard_map/all_gather | solution.py:129
  32.3 2.1 fusion.48
  36.4 3.5 %collective-permute-start = (bf16[3,1,256]{2,1,0:T(2,128)(2,1)S(1)}, bf16[3,1,256]{2,1,0:T(2,128)(2,1)S(1)}, u32[]{:S(2)}, u32[]{:S(2)}) collective-permute-start(bf16[3,1,256]{2,1,0:T(2,128)(2,1)S(1)} %slice.58), channel_id=1, source_target_pairs={{0,4},{4,8},{8,12},{12,16},{16,20},{20,24},{24,28},{1,5},{5,9},{9,... | collective-permute-start | bytes 4616 | tf_op jit(solution)/shard_map/ppermute | solution.py:16
  40.0 1.6 fusion.81
  42.2 1.3 reshape.65
  43.4 1.3 log.10
  44.8 1.1 copy.125
  45.9 1.8 reduce_window_sum.11
  47.8 1.2 fusion.28
  48.9 1.1 fusion.89
  50.3 1.3 reshape_squeeze.10
  51.7 2.0 bitcast_divide_fusion.1
  53.8 2.4 convolution_select_fusion.2
  56.2 1.4 fusion.26
  57.6 118.6 %custom-call.4 = f32[6,4,1,64,64]{3,4,2,1,0:T(8,128)} custom-call(f32[6,4,1,64,64]{4,3,2,1,0:T(8,128)S(1)} %fusion.26), custom_call_target="InvertDiagBlocksLowerTriangular" | custom-call | tf_op jit(solution)/shard_map/jit(_solve_triangular)/vmap(vmap())/triangular_solve | solution.py:66
  176.2 1.3 reshape_squeeze.11
  178.5 2.2 fusion.61
  180.7 1.6 fusion.55
  182.3 2.3 convolution_add_fusion.4
  184.6 2.6 fusion.67
  187.2 2.2 reshape_squeeze.12
  189.4 2.7 convolution_select_fusion.1
  192.2 1.5 convolution_select_fusion
  193.7 1.9 convolution_add_fusion.2
  196.9 1.7 convolution_add_fusion.3
  200.5 18.9 %while.28 = (s32[]{:T(128)}, f32[4,128,64]{1,2,0:T(8,128)S(1)}, f32[6,4,64,128]{3,2,1,0:T(8,128)}, f32[6,4,64,64]{3,2,1,0:T(8,128)}, f32[6,4,128,64]{2,3,1,0:T(8...) while((s32[]{:T(128)}, f32[4,128,64]{1,2,0:T(8,128)S(1)}, ...), condition=%wide.region_4.5_spmd, body=%wide.region_3.4_spmd.sunk | while | flops 50397184 | bytes 1312861 | solution.py:102
  200.5 1.8 fusion.138
  202.3 1.3 fusion.137
  203.6 1.8 fusion.138
  205.5 1.3 fusion.137
  206.8 1.8 fusion.138
  208.6 1.3 fusion.137
  210.0 1.8 fusion.138
  211.8 1.3 fusion.137
  213.1 1.8 fusion.138
  214.9 1.3 fusion.137
  216.2 1.8 fusion.138
  218.1 1.3 fusion.137
  219.5 34.8 %all-gather.1 = f32[32,64,64]{2,1,0:T(8,128)} all-gather(f32[4,64,64]{2,1,0:T(8,128)S(1)} %get-tuple-element.240), channel_id=3, replica_groups=mesh['sp'=8,'tp'=4] {'sp'}, dimensions={0}, use_global_device_ids=true | all-gather | bytes 589824 | tf_op jit(solution)/shard_map/all_gather | solution.py:21
  254.4 32.6 %all-gather = f32[32,64,64]{2,1,0:T(8,128)S(1)} all-gather(f32[4,64,64]{2,1,0:T(8,128)S(1)} %get-tuple-element.241), channel_id=2, replica_groups=mesh['sp'=8,'tp'=4] {'sp'}, dimensions={0}, use_global_device_ids=true | all-gather | bytes 589824 | tf_op jit(solution)/shard_map/all_gather | solution.py:21
  287.0 13.2 %while.29 = (s32[]{:T(128)}, f32[4,64,64]{1,2,0:T(8,128)S(1)}, f32[4,64,64]{1,2,0:T(8,128)S(1)}, s32[]{:T(128)}, f32[8,4,64,64]{3,2,1,0:T(8,128)S(1)}, /*index=5*/f32[8,4,64,64]{3,2,1,0:T(8,128)}, s32[]{:T(128)}, s32[]{:T(128)}) while((s32[]{:T(128)}, f32[4,64,64]{1,2,0:T(8,128)S(1)}, f32[4,64,64]{1,2,0:T(8,128)S(1)}, s32[]{:T(128)}, ...), condition=%wide.region_6.7_spmd.clone, body=%wide.region_5.6_spmd.clone.sunk | while | flops 25247748 | bytes 1575032 | solution.py:30
  300.2 1.6 copy.66
  302.2 3.7 %fusion.91 = (f32[6,4,64]{2,0,1:T(8,128)S(1)}, f32[6,4,64,64]{2,3,0,1:T(8,128)S(1)}) fusion(f32[4,64,64,1]{1,2,3,0:T(8,128)S(1)} %fusion.50, f32[6,4,64,128]{2,3,0,1:T(8,128)S(1)} %copy.66, f32[6,4,64,128]{3,2,1,0:T(8,128)} %get-tuple-element.153), kind=kOutput, calls=%fused_computation.138 | convolution fusion | flops 75692544 | bytes 1644544 | tf_op jit(solution)/shard_map/bhtj,hvj->bhtv/dot_general | solution.py:182
  307.0 2.4 fusion.35
  309.5 7.7 %all_to_all.19 = bf16[4,96,256]{2,1,0:T(8,128)(2,1)S(1)} all-to-all(bf16[4,96,256]{2,1,0:T(8,128)(2,1)S(1)} %bitcast.170), channel_id=1, replica_groups=mesh['sp'=8,'tp'=4] {'tp'}, dimensions={0} | all-to-all | bytes 393216 | tf_op jit(solution)/shard_map/all_to_all | solution.py:191
  317.2 1.6 convolution_convert_fusion
  (154 shorter events, 24.9 us)
Async XLA Ops:
  6.5 25.7 %copy-start = (bf16[2048,256]{1,0:T(8,128)(2,1)S(1)}, bf16[2048,256]{1,0:T(8,128)(2,1)}, u32[]{:S(2)}) copy-start(bf16[2048,256]{1,0:T(8,128)(2,1)} %param.23) | copy-start | bytes 3145732
  6.5 3.3 %copy-start.24 = (f32[256]{0:T(256)S(1)}, f32[256]{0:T(256)}, u32[]{:S(2)}) copy-start(f32[256]{0:T(256)} %param.31) | copy-start | bytes 3076
  6.5 25.7 %all-gather.4.cloned.1.call-start = ((), (), s32[]{:S(2)}) async-start(), calls=%async_computation.1 | async-start | bytes 1966080 | tf_op jit(solution)/shard_map/all_gather | solution.py:129
  10.5 0.6 copy-start.15
  13.2 21.2 %copy-start.26 = (bf16[2048,256]{1,0:T(8,128)(2,1)S(1)}, bf16[2048,256]{1,0:T(8,128)(2,1)}, u32[]{:S(2)}) copy-start(bf16[2048,256]{1,0:T(8,128)(2,1)} %param.22) | copy-start | bytes 3145732
  32.3 2.1 copy-start.25
  34.4 1.2 copy-start.27
  36.2 5.4 %copy-start.13 = (bf16[1,384,256]{2,1,0:T(8,128)(2,1)}, bf16[1,384,256]{2,1,0:T(8,128)(2,1)S(1)}, u32[]{:S(2)}) copy-start(bf16[1,384,256]{2,1,0:T(8,128)(2,1)S(1)} %fusion.46) | copy-start | bytes 589828
  36.2 3.7 %copy-start.28 = (bf16[2048,256]{1,0:T(8,128)(2,1)S(1)}, bf16[2048,256]{1,0:T(8,128)(2,1)}, u32[]{:S(2)}) copy-start(bf16[2048,256]{1,0:T(8,128)(2,1)} %param.24) | copy-start | bytes 3145732
  36.2 3.7 %copy-start.30 = (f32[384]{0:T(512)S(1)}, f32[384]{0:T(512)}, u32[]{:S(2)}) copy-start(f32[384]{0:T(512)} %param.30) | copy-start | bytes 4612
  36.3 3.7 %copy-start.31 = (f32[256]{0:T(256)S(1)}, f32[256]{0:T(256)}, u32[]{:S(2)}) copy-start(f32[256]{0:T(256)} %param.28) | copy-start | bytes 3076
  36.4 5.2 %copy-start.29 = (bf16[2048,256]{1,0:T(8,128)(2,1)S(1)}, bf16[2048,256]{1,0:T(8,128)(2,1)}, u32[]{:S(2)}) copy-start(bf16[2048,256]{1,0:T(8,128)(2,1)} %param.25) | copy-start | bytes 3145732
  36.4 5.2 %copy-start.32 = (f32[256]{0:T(256)S(1)}, f32[256]{0:T(256)}, u32[]{:S(2)}) copy-start(f32[256]{0:T(256)} %param.29) | copy-start | bytes 3076
  36.4 11.3 %collective-permute-start = (bf16[3,1,256]{2,1,0:T(2,128)(2,1)S(1)}, bf16[3,1,256]{2,1,0:T(2,128)(2,1)S(1)}, u32[]{:S(2)}, u32[]{:S(2)}) collective-permute-start(bf16[3,1,256]{2,1,0:T(2,128)(2,1)S(1)} %slice.58), channel_id=1, source_target_pairs={{0,4},{4,8},{8,12},{12,16},{16,20},{20,24},{24,28},{1,5},{5,9},{9,... | collective-permute-start | bytes 4616 | tf_op jit(solution)/shard_map/ppermute | solution.py:16
  44.8 1.1 copy-start.5
  44.8 3.0 copy-start.23
  51.7 2.1 copy-start.3
  51.7 2.1 copy-start.21
  53.7 2.5 copy-start.6
  53.8 2.5 copy-start.16
  53.8 2.4 copy-start.18
  53.8 2.4 copy-start.22
  177.6 0.9 copy-start.1
  178.5 2.2 copy-start.7
  178.5 2.2 copy-start.14
  180.7 1.6 copy-start.17
  189.4 2.7 copy-start.4
  189.4 2.7 copy-start.8
  189.4 2.7 copy-start.20
  195.5 1.1 copy-start.2
  195.5 1.4 copy-start.12
  199.6 0.9 copy-start.9
  219.4 67.6 %copy-start.10 = (f32[4,64,64]{1,2,0:T(8,128)S(1)}, f32[4,64,64]{1,2,0:T(8,128)}, u32[]{:S(2)}) copy-start(f32[4,64,64]{1,2,0:T(8,128)} %custom-call.5) | copy-start | bytes 196612
  300.2 1.7 copy-start.19
  307.0 10.1 %copy-start.11 = (bf16[1024,2048]{1,0:T(8,128)(2,1)S(1)}, bf16[1024,2048]{1,0:T(8,128)(2,1)}, u32[]{:S(2)}) copy-start(bf16[1024,2048]{1,0:T(8,128)(2,1)} %param.33) | copy-start | bytes 12582916
Sparse Core Ops, SparseCore 0:
  9.9 22.3 all-gather.3
where the time goes:
time: 327 us; the launch traced here: 326 us
  other arithmetic  130 us (40%)
  blocking collectives  75.1 us (23%)
  matrix products  59.8 us (18%)
  local copies, waits for them, and re-layouts  23.2 us (7%)
  waiting for transfers between devices  19.1 us (6%)
  between operations  14 us (4%)
  starting transfers between devices  3.5 us (1%)
    another operation x2, other arithmetic, prepare_blocks(): jax.scipy.linalg.solve_triangular(system, targets, lower=True, unit_diago...  119 us
    all_gather x2, blocking collectives, carried_in(): pieces = jax.tree.map(lambda part: lax.all_gather(part, axis), value)  67.4 us
    all_gather x1, waiting for transfers between devices, per_device(): piece = lax.all_gather(normed, 'tp', axis=0, tiled=True)  19.1 us
    dot_general x6, matrix products, block_step(): jnp.einsum('htn,hrn->htr', reads_now, state, precision=highest) + fixed_now  10.9 us
    dot_general x4, matrix products, pair_dots(): return jnp.einsum('bhtn,bhsn->bhts', left, right, precision=highest)  8.01 us
    dot_general x6, matrix products, per_device(): jnp.dot(piece, weight, preferred_element_type=jnp.float32)  7.88 us
    dot_general x6, matrix products, block_step(): jnp.einsum('hrm,hmn->hrn', state, trans_now, precision=highest) + added_now  7.73 us
    all_to_all x1, blocking collectives, per_device(): lax.all_to_all(gated, 'tp', split_axis=0, concat_axis=1, tiled=True)  7.67 us
  transfers between devices with their start and end apart: 2, of which 1 were waited for; matrix products, arithmetic and copies ran while one was open for 3% of the time, Pallas kernels for 0%

commit v1 on v0

--- a/solution.py
+++ b/solution.py
@@ -126,7 +126,12 @@
         * norm_gain
     ).astype(jnp.bfloat16)
     weights = (w_recept, w_key, w_value, w_decay, w_rate, w_gate)
-    piece = lax.all_gather(normed, "tp", axis=0, tiled=True)
+    ring = [normed]
+    for hop in range(3):
+        ring.append(lax.ppermute(ring[-1], "tp", [(dev, (dev + 1) % 4) for dev in range(4)]))
+    piece = jnp.roll(
+        jnp.concatenate(ring[::-1], axis=0), (lax.axis_index("tp") + 1) * ring[0].shape[0], axis=0
+    )
     projected = jnp.stack(
         [
             jnp.dot(piece, weight, preferred_element_type=jnp.float32).astype(jnp.bfloat16)

time: 327 us -> 314 us (0.960)
  between operations: 14 us -> 0.67 us
    all_gather x1 -> x0, waiting for transfers between devices: 19.1 us -> none  [per_device(): piece = lax.all_gather(normed, 'tp', axis=0, tiled=True)]
    ppermute x0 -> x3, waiting for transfers between devices: none -> 17.7 us  [per_device(): lax.ppermute(ring[-1], 'tp', [(dev, (dev + 1) % 4) for dev in range(4)])]
  transfers between devices with their start and end apart: 2 -> 4, of which waited for: 1 -> 3; matrix products, arithmetic and copies ran while one was open for 3% -> 4% of each run, Pallas kernels for 0% -> 0%
where the time goes in v1:
time: 314 us; the launch traced here: 313 us
  other arithmetic  130 us (41%)
  blocking collectives  76.1 us (24%)
  matrix products  59.5 us (19%)
  local copies, waits for them, and re-layouts  23.2 us (7%)
  waiting for transfers between devices  17.7 us (6%)
  starting transfers between devices  4.86 us (2%)
    another operation x2, other arithmetic, prepare_blocks(): jax.scipy.linalg.solve_triangular(system, targets, lower=True, unit_diago...  119 us
    all_gather x2, blocking collectives, carried_in(): pieces = jax.tree.map(lambda part: lax.all_gather(part, axis), value)  68.5 us
    ppermute x3, waiting for transfers between devices, per_device(): lax.ppermute(ring[-1], 'tp', [(dev, (dev + 1) % 4) for dev in range(4)])  17.7 us
    dot_general x6, matrix products, block_step(): jnp.einsum('htn,hrn->htr', reads_now, state, precision=highest) + fixed_now  11 us
    dot_general x4, matrix products, pair_dots(): return jnp.einsum('bhtn,bhsn->bhts', left, right, precision=highest)  7.94 us
    dot_general x6, matrix products, block_step(): jnp.einsum('hrm,hmn->hrn', state, trans_now, precision=highest) + added_now  7.73 us
    all_to_all x1, blocking collectives, per_device(): lax.all_to_all(gated, 'tp', split_axis=0, concat_axis=1, tiled=True)  7.67 us
    dynamic_slice x14, local copies, waits for them, and re-layouts, turn(): longer = join(running, jax.tree.map(lambda part: part[position], pieces))  7.11 us
  transfers between devices with their start and end apart: 4, of which 3 were waited for; matrix products, arithmetic and copies ran while one was open for 4% of the time, Pallas kernels for 0%

profile of v1, /device:TPU:0, one launch (start us, length us, event | category | flops | bytes accessed | tf_op | source)
XLA Modules:
  0.0 312.6 jit_solution(15672159589248534829)
XLA Ops:
  0.0 1.3 fusion.51
  1.3 1.2 fusion.53
  3.0 7.4 %collective-permute-done = bf16[96,2048]{1,0:T(8,128)(2,1)S(1)} collective-permute-done((bf16[96,2048]{1,0:T(8,128)(2,1)S(1)}, bf16[96,2048]{1,0:T(8,128)(2,1)S(1)}, u32[]{:S(2)}, u32[]{:S(2)}) %collective-permute-start) | collective-permute-done | bytes 393248 | tf_op jit(solution)/shard_map/ppermute | solution.py:131
  13.2 4.4 %collective-permute-done.1 = bf16[96,2048]{1,0:T(8,128)(2,1)S(1)} collective-permute-done((bf16[96,2048]{1,0:T(8,128)(2,1)S(1)}, bf16[96,2048]{1,0:T(8,128)(2,1)S(1)}, u32[]{:S(2)}, u32[]{:S(2)}) %collective-permute-start.1) | collective-permute-done | bytes 393248 | tf_op jit(solution)/shard_map/ppermute | solution.py:131
  18.9 5.9 %collective-permute-done.2 = bf16[96,2048]{1,0:T(8,128)(2,1)S(1)} collective-permute-done((bf16[96,2048]{1,0:T(8,128)(2,1)S(1)}, bf16[96,2048]{1,0:T(8,128)(2,1)S(1)}, u32[]{:S(2)}, u32[]{:S(2)}) %collective-permute-start.2) | collective-permute-done | bytes 393248 | tf_op jit(solution)/shard_map/ppermute | solution.py:131
  28.3 4.3 %collective-permute-start.3 = (bf16[3,1,256]{2,1,0:T(2,128)(2,1)S(1)}, bf16[3,1,256]{2,1,0:T(2,128)(2,1)S(1)}, u32[]{:S(2)}, u32[]{:S(2)}) collective-permute-start(bf16[3,1,256]{2,1,0:T(2,128)(2,1)S(1)} %slice.58), channel_id=1, source_target_pairs={{0,4},{4,8},{8,12},{12,16},{16,20},{20,24},{24,28},{1,5},{5,9},{9,... | collective-permute-start | bytes 4616 | tf_op jit(solution)/shard_map/ppermute | solution.py:16
  32.7 1.6 fusion.87
  34.9 1.2 reshape.65
  36.1 1.3 log.10
  37.5 1.2 copy.125
  38.6 1.8 reduce_window_sum.11
  40.5 1.2 fusion.28
  43.1 1.3 reshape_squeeze.10
  44.4 2.0 bitcast_divide_fusion.1
  46.5 2.4 convolution_select_fusion.2
  48.9 1.4 fusion.26
  50.3 118.6 %custom-call.4 = f32[6,4,1,64,64]{3,4,2,1,0:T(8,128)} custom-call(f32[6,4,1,64,64]{4,3,2,1,0:T(8,128)S(1)} %fusion.26), custom_call_target="InvertDiagBlocksLowerTriangular" | custom-call | tf_op jit(solution)/shard_map/jit(_solve_triangular)/vmap(vmap())/triangular_solve | solution.py:66
  168.9 1.3 reshape_squeeze.11
  171.1 2.1 fusion.61
  173.2 3.0 fusion.55
  176.2 2.3 convolution_add_fusion.4
  178.5 2.5 fusion.67
  181.0 2.3 reshape_squeeze.12
  183.3 2.7 convolution_select_fusion.1
  186.0 1.5 convolution_select_fusion
  187.5 1.9 convolution_add_fusion.2
  190.4 1.7 convolution_add_fusion.3
  193.3 18.9 %while.28 = (s32[]{:T(128)}, f32[4,128,64]{1,2,0:T(8,128)S(1)}, f32[6,4,64,128]{3,2,1,0:T(8,128)}, f32[6,4,64,64]{3,2,1,0:T(8,128)}, f32[6,4,128,64]{2,3,1,0:T(8...) while((s32[]{:T(128)}, f32[4,128,64]{1,2,0:T(8,128)S(1)}, ...), condition=%wide.region_4.5_spmd, body=%wide.region_3.4_spmd.sunk | while | flops 50397184 | bytes 1312861 | solution.py:102
  193.3 1.8 fusion.146
  195.1 1.3 fusion.145
  196.5 1.8 fusion.146
  198.3 1.3 fusion.145
  199.6 1.8 fusion.146
  201.5 1.3 fusion.145
  202.8 1.8 fusion.146
  204.6 1.3 fusion.145
  205.9 1.8 fusion.146
  207.8 1.3 fusion.145
  209.1 1.8 fusion.146
  210.9 1.3 fusion.145
  212.4 35.4 %all-gather.1 = f32[32,64,64]{2,1,0:T(8,128)} all-gather(f32[4,64,64]{2,1,0:T(8,128)S(1)} %get-tuple-element.240), channel_id=3, replica_groups=mesh['sp'=8,'tp'=4] {'sp'}, dimensions={0}, use_global_device_ids=true | all-gather | bytes 589824 | tf_op jit(solution)/shard_map/all_gather | solution.py:21
  247.8 33.1 %all-gather = f32[32,64,64]{2,1,0:T(8,128)S(1)} all-gather(f32[4,64,64]{2,1,0:T(8,128)S(1)} %get-tuple-element.241), channel_id=2, replica_groups=mesh['sp'=8,'tp'=4] {'sp'}, dimensions={0}, use_global_device_ids=true | all-gather | bytes 589824 | tf_op jit(solution)/shard_map/all_gather | solution.py:21
  280.9 13.2 %while.29 = (s32[]{:T(128)}, f32[4,64,64]{1,2,0:T(8,128)S(1)}, f32[4,64,64]{1,2,0:T(8,128)S(1)}, s32[]{:T(128)}, f32[8,4,64,64]{3,2,1,0:T(8,128)S(1)}, /*index=5*/f32[8,4,64,64]{3,2,1,0:T(8,128)}, s32[]{:T(128)}, s32[]{:T(128)}) while((s32[]{:T(128)}, f32[4,64,64]{1,2,0:T(8,128)S(1)}, f32[4,64,64]{1,2,0:T(8,128)S(1)}, s32[]{:T(128)}, ...), condition=%wide.region_6.7_spmd.clone, body=%wide.region_5.6_spmd.clone.sunk | while | flops 25247748 | bytes 1575032 | solution.py:30
  294.1 1.6 copy.66
  296.1 3.7 %fusion.105 = (f32[6,4,64]{2,0,1:T(8,128)S(1)}, f32[6,4,64,64]{2,3,0,1:T(8,128)S(1)}) fusion(f32[4,64,64,1]{1,2,3,0:T(8,128)S(1)} %fusion.50, f32[6,4,64,128]{2,3,0,1:T(8,128)S(1)} %copy.66, f32[6,4,64,128]{3,2,1,0:T(8,128)} %get-tuple-element.153), kind=kOutput, calls=%fused_computation.158 | convolution fusion | flops 75692544 | bytes 1644544 | tf_op jit(solution)/shard_map/bhtj,hvj->bhtv/dot_general | solution.py:187
  300.9 2.5 fusion.35
  303.3 7.7 %all_to_all.19 = bf16[4,96,256]{2,1,0:T(8,128)(2,1)S(1)} all-to-all(bf16[4,96,256]{2,1,0:T(8,128)(2,1)S(1)} %bitcast.164), channel_id=1, replica_groups=mesh['sp'=8,'tp'=4] {'tp'}, dimensions={0} | all-to-all | bytes 393216 | tf_op jit(solution)/shard_map/all_to_all | solution.py:196
  311.0 1.6 convolution_convert_fusion
  (163 shorter events, 27.4 us)
Async XLA Ops:
  0.0 25.4 %copy-start = (bf16[2048,256]{1,0:T(8,128)(2,1)S(1)}, bf16[2048,256]{1,0:T(8,128)(2,1)}, u32[]{:S(2)}) copy-start(bf16[2048,256]{1,0:T(8,128)(2,1)} %param.21) | copy-start | bytes 3145732
  0.0 24.9 %copy-start.9 = (bf16[96,2048]{1,0:T(8,128)(2,1)S(1)}, bf16[96,2048]{1,0:T(8,128)(2,1)}, u32[]{:S(2)}) copy-start(bf16[96,2048]{1,0:T(8,128)(2,1)} %param.19) | copy-start | bytes 1179652
  0.0 24.9 %copy-start.19 = (f32[2048]{0:T(1024)S(1)}, f32[2048]{0:T(1024)}, u32[]{:S(2)}) copy-start(f32[2048]{0:T(1024)} %param.20) | copy-start | bytes 24580
  2.5 8.0 %collective-permute-start = (bf16[96,2048]{1,0:T(8,128)(2,1)S(1)}, bf16[96,2048]{1,0:T(8,128)(2,1)S(1)}, u32[]{:S(2)}, u32[]{:S(2)}) collective-permute-start(bf16[96,2048]{1,0:T(8,128)(2,1)S(1)} %fusion.53), channel_id=1, source_target_pairs={{0,1},{1,2},{2,3},{3,0},{4,5},{5,6},{6,7},{7,4},{8,9},{9,10},{10,1... | collective-permute-start | bytes 1179656 | tf_op jit(solution)/shard_map/ppermute | solution.py:131
  10.4 7.2 %collective-permute-start.1 = (bf16[96,2048]{1,0:T(8,128)(2,1)S(1)}, bf16[96,2048]{1,0:T(8,128)(2,1)S(1)}, u32[]{:S(2)}, u32[]{:S(2)}) collective-permute-start(bf16[96,2048]{1,0:T(8,128)(2,1)S(1)} %collective-permute-done), channel_id=1, source_target_pairs={{0,1},{1,2},{2,3},{3,0},{4,5},{5,6},{6,7},{7,4},{8,9},{9,10},{10,1... | collective-permute-start | bytes 1179656 | tf_op jit(solution)/shard_map/ppermute | solution.py:131
  11.8 0.6 copy-start.14
  17.6 7.2 %collective-permute-start.2 = (bf16[96,2048]{1,0:T(8,128)(2,1)S(1)}, bf16[96,2048]{1,0:T(8,128)(2,1)S(1)}, u32[]{:S(2)}, u32[]{:S(2)}) collective-permute-start(bf16[96,2048]{1,0:T(8,128)(2,1)S(1)} %collective-permute-done.1), channel_id=1, source_target_pairs={{0,1},{1,2},{2,3},{3,0},{4,5},{5,6},{6,7},{7,4},{8,9},{9,10},{10,1... | collective-permute-start | bytes 1179656 | tf_op jit(solution)/shard_map/ppermute | solution.py:131
  25.1 1.3 copy-start.25
  25.4 8.9 %copy-start.20 = (bf16[768,2048]{1,0:T(8,128)(2,1)}, bf16[768,2048]{1,0:T(8,128)(2,1)S(1)}, u32[]{:S(2)}) copy-start(bf16[768,2048]{1,0:T(8,128)(2,1)S(1)} %constant_dynamic-update-slice_fusion) | copy-start | bytes 9437188
  25.4 2.1 copy-start.26
  27.5 5.1 %copy-start.27 = (bf16[2048,256]{1,0:T(8,128)(2,1)S(1)}, bf16[2048,256]{1,0:T(8,128)(2,1)}, u32[]{:S(2)}) copy-start(bf16[2048,256]{1,0:T(8,128)(2,1)} %param.24) | copy-start | bytes 3145732
  27.5 5.1 %copy-start.29 = (f32[384]{0:T(512)S(1)}, f32[384]{0:T(512)}, u32[]{:S(2)}) copy-start(f32[384]{0:T(512)} %param.30) | copy-start | bytes 4612
  27.5 5.1 %copy-start.30 = (f32[256]{0:T(256)S(1)}, f32[256]{0:T(256)}, u32[]{:S(2)}) copy-start(f32[256]{0:T(256)} %param.28) | copy-start | bytes 3076
  28.1 6.1 %copy-start.13 = (bf16[1,384,256]{2,1,0:T(8,128)(2,1)}, bf16[1,384,256]{2,1,0:T(8,128)(2,1)S(1)}, u32[]{:S(2)}) copy-start(bf16[1,384,256]{2,1,0:T(8,128)(2,1)S(1)} %fusion.48) | copy-start | bytes 589828
  28.1 6.1 %copy-start.28 = (bf16[2048,256]{1,0:T(8,128)(2,1)S(1)}, bf16[2048,256]{1,0:T(8,128)(2,1)}, u32[]{:S(2)}) copy-start(bf16[2048,256]{1,0:T(8,128)(2,1)} %param.25) | copy-start | bytes 3145732
  28.2 6.1 %copy-start.31 = (f32[256]{0:T(256)S(1)}, f32[256]{0:T(256)}, u32[]{:S(2)}) copy-start(f32[256]{0:T(256)} %param.29) | copy-start | bytes 3076
  28.3 12.2 %collective-permute-start.3 = (bf16[3,1,256]{2,1,0:T(2,128)(2,1)S(1)}, bf16[3,1,256]{2,1,0:T(2,128)(2,1)S(1)}, u32[]{:S(2)}, u32[]{:S(2)}) collective-permute-start(bf16[3,1,256]{2,1,0:T(2,128)(2,1)S(1)} %slice.58), channel_id=1, source_target_pairs={{0,4},{4,8},{8,12},{12,16},{16,20},{20,24},{24,28},{1,5},{5,9},{9,... | collective-permute-start | bytes 4616 | tf_op jit(solution)/shard_map/ppermute | solution.py:16
  34.9 5.6 %copy-start.24 = (f32[3,256]{1,0:T(4,128)S(1)}, f32[3,256]{1,0:T(4,128)}, u32[]{:S(2)}) copy-start(f32[3,256]{1,0:T(4,128)} %param.27) | copy-start | bytes 9220
  37.5 1.2 copy-start.5
  44.4 4.5 %copy-start.3 = (f32[6,64,4,64]{3,2,1,0:T(4,128)}, f32[6,64,4,64]{3,2,1,0:T(4,128)S(1)}, u32[]{:S(2)}) copy-start(f32[6,64,4,64]{3,2,1,0:T(4,128)S(1)} %reshape_squeeze.10) | copy-start | bytes 1179652
  44.4 2.1 copy-start.22
  46.4 2.4 copy-start.6
  46.5 2.4 copy-start.15
  46.5 2.4 copy-start.17
  46.5 2.4 copy-start.23
  170.3 0.9 copy-start.1
  171.1 5.1 %copy-start.16 = (f32[64,64]{1,0:T(8,128)S(1)}, f32[64,64]{1,0:T(8,128)}, u32[]{:S(2)}) copy-start(f32[64,64]{1,0:T(8,128)} %copy-done.14) | copy-start | bytes 49156
  183.3 2.7 copy-start.4
  183.3 2.7 copy-start.7
  183.3 2.7 copy-start.21
  187.5 2.9 copy-start.2
  187.5 2.9 copy-start.12
  192.2 1.1 copy-start.8
  212.2 68.6 %copy-start.10 = (f32[4,64,64]{1,2,0:T(8,128)S(1)}, f32[4,64,64]{1,2,0:T(8,128)}, u32[]{:S(2)}) copy-start(f32[4,64,64]{1,2,0:T(8,128)} %custom-call.5) | copy-start | bytes 196612
  280.9 14.8 %copy-start.18 = (f32[4,64,64]{2,1,0:T(8,128)S(1)}, f32[4,64,64]{2,1,0:T(8,128)}, u32[]{:S(2)}) copy-start(f32[4,64,64]{2,1,0:T(8,128)} %param.32) | copy-start | bytes 196612
  300.9 10.2 %copy-start.11 = (bf16[1024,2048]{1,0:T(8,128)(2,1)S(1)}, bf16[1024,2048]{1,0:T(8,128)(2,1)}, u32[]{:S(2)}) copy-start(bf16[1024,2048]{1,0:T(8,128)(2,1)} %param.33) | copy-start | bytes 12582916
